TPU v7x, 32 devices: a whole 2x2x4 slice. The times are simulated.
32 devices in a mesh: sp: 16 (over z, y, x), tp: 2 (over core).
Axes of the slice: x: 2, y: 2, z: 4, core: 2. Of those that a mesh axis runs over, the one named last changes fastest.
Arguments:
- tokens: bfloat16 [4096, 2048], P('sp', 'tp'), may hold values from -6 to 6
- norm_gain: float32 [2048], replicated, may hold values from 0.1 to 1.9
- recur_query: bfloat16 [2048, 1024], P(None, 'tp'), may hold values from -0.125 to 0.125
- recur_forget: bfloat16 [2048, 1024], P(None, 'tp'), may hold values from -0.125 to 0.125
- recur_value: bfloat16 [2048, 1024], P(None, 'tp'), may hold values from -0.125 to 0.125
- gate_floor: float32 [1024], P('tp'), may hold values from 0.5 to 1
- extra_decay: float32 [4096, 8], P('sp', 'tp'), may hold values from 0 to 2
- start_state: float32 [8, 128, 128], P('tp'), may hold values from -0.125 to 0.125
- recur_gain: float32 [1024], P('tp'), may hold values from 0.1 to 1.9
- attend_query: bfloat16 [2048, 1024], P(None, 'tp')
- attend_key: bfloat16 [2048, 1024], P(None, 'tp')
- attend_value: bfloat16 [2048, 1024], P(None, 'tp'), may hold values from -0.125 to 0.125
- gate_cache: float32 [4096, 16], P(None, 'tp'), may hold values from -4096 to 0, as said below
- attend_gain: float32 [1024], P('tp'), may hold values from 0.1 to 1.9
- recur_output: bfloat16 [1024, 2048], P(None, 'tp'), may hold values from -0.1875 to 0.1875
- attend_output: bfloat16 [1024, 2048], P(None, 'tp'), may hold values from -0.1875 to 0.1875
Outputs:
- layer_output: bfloat16 [4096, 2048], P('sp', 'tp')
Inputs may be any that keep to these rules, and one draw needn't show every extreme that they name: `gate_cache`: never rising along positions.
All inputs are finite; a program needn't handle non-finite values.
Results may differ from a plain program's by a relative error of at most 0.018.
Values may be sent and summed in bfloat16 or wider, within the bound.
A program may use at most 64 MiB of HBM per device.

v0:
```python
import jax
import jax.numpy as jnp
from jax import lax
from jax.sharding import PartitionSpec as P

FD = 64


EPSILON = 1e-06
TOP_PRECISION = lax.Precision.HIGHEST


def prefix(x, axis, combine, identity):
    devices, position = (lax.axis_size(axis), lax.axis_index(axis))
    everything = jax.tree.map(
        lambda part, kind: lax.all_gather(part.astype(kind), axis), x, (jnp.bfloat16, jnp.bfloat16)
    )
    start = jax.tree.map(
        lambda part, zero: jnp.broadcast_to(jnp.asarray(zero, part.dtype), part.shape), x, identity
    )

    def step(k, before):
        reached = k < position
        new = combine(
            before, jax.tree.map(lambda part, own: part[k].astype(own.dtype), everything, x)
        )
        return jax.tree.map(lambda a, b: jnp.where(reached, a, b), new, before)

    return lax.fori_loop(0, devices, step, start)


def head_norm(per_head, head_gain):
    normed = per_head * lax.rsqrt(jnp.mean(per_head * per_head, axis=-1, keepdims=True) + EPSILON)
    return normed.reshape(per_head.shape[0], -1) * head_gain


def local_recurrence(query_rows, decays, inflow, values):
    span_len = min(64, query_rows.shape[0])
    blocks = query_rows.shape[0] // span_len

    def to_blocks(tensor):
        return tensor.reshape(blocks, span_len, tensor.shape[1], tensor.shape[2])

    causal = jnp.tril(jnp.ones((span_len, span_len), dtype=bool))[:, :, None, None]

    def advance(carried_state, pieces):
        query_block, g_block, k_block, value_block = pieces
        running_total = jnp.cumsum(g_block, axis=0)
        offsets = jnp.where(causal, running_total[:, None] - running_total[None, :], -jnp.inf)
        mixing = jnp.einsum(
            "thk,shk,tshk->hts", query_block, k_block, jnp.exp(offsets), precision=TOP_PRECISION
        )
        final_result = jnp.einsum("hts,shv->thv", mixing, value_block, precision=TOP_PRECISION)
        final_result = final_result + jnp.einsum(
            "dzc,zcu->dzu",
            query_block * jnp.exp(running_total),
            carried_state,
            precision=TOP_PRECISION,
        )
        ending_state = running_total[-1]
        weighted_values = k_block * jnp.exp(ending_state[None] - running_total)
        carried_state = jnp.exp(ending_state)[..., None] * carried_state + jnp.einsum(
            "cun,cub->unb", weighted_values, value_block, precision=TOP_PRECISION
        )
        return (carried_state, final_result)

    initial = jnp.zeros((query_rows.shape[1], query_rows.shape[2], values.shape[2]), jnp.float32)
    final_state, results = lax.scan(
        advance,
        initial,
        (to_blocks(query_rows), to_blocks(decays), to_blocks(inflow), to_blocks(values)),
    )
    return (results.reshape(query_rows.shape[0], query_rows.shape[1], values.shape[2]), final_state)


def keep_state(running_state):
    return running_state


def block_update(
    group_query, group_gates, group_index, key_rows, value_rows, key_gates, key_index, scaling
):

    def compute(running_state):
        maxima, totals, summed = running_state
        scores = (
            jnp.einsum("qhd,khd->hqk", group_query, key_rows, preferred_element_type=jnp.float32)
            * scaling
        )
        scores = scores + group_gates.T[:, :, None] - key_gates.T[:, None, :]
        allowed = (key_index[None, :] <= group_index[:, None])[None]
        highest = jnp.maximum(maxima, jnp.max(jnp.where(allowed, scores, -1e30), axis=-1))
        weights = jnp.where(allowed, jnp.exp(scores - highest[..., None]), 0.0)
        rescale = jnp.exp(maxima - highest)
        totals = totals * rescale + jnp.sum(weights, axis=-1)
        summed = summed * rescale.T[:, :, None] + jnp.einsum(
            "hqk,khd->qhd",
            weights.astype(jnp.bfloat16),
            value_rows,
            preferred_element_type=jnp.float32,
        )
        return (highest, totals, summed)

    return compute


def shards(
    tokens,
    norm_gain,
    recur_query,
    recur_forget,
    recur_value,
    gate_floor,
    extra_decay,
    start_state,
    recur_gain,
    attend_query,
    attend_key,
    attend_value,
    gate_cache,
    attend_gain,
    recur_output,
    attend_output,
):
    height = tokens.shape[0]
    model_width = norm_gain.shape[0]
    inputs = (recur_query, recur_forget, recur_value, attend_query, attend_key, attend_value)
    wide = lax.all_gather(tokens, "tp", axis=1, tiled=True).astype(jnp.float32)
    scaled = (wide * norm_gain).astype(jnp.bfloat16)
    updated = tuple(
        (jnp.dot(scaled, weight, preferred_element_type=jnp.float32) for weight in inputs)
    )
    products = updated
    squares = jnp.sum(wide * wide, axis=1, keepdims=True)
    inverse = lax.rsqrt(squares / model_width + EPSILON)
    projected = tuple(
        ((partial_value * inverse).astype(jnp.bfloat16) for partial_value in products)
    )
    rec_heads = start_state.shape[0]
    query_rows = projected[0].astype(jnp.float32).reshape(height, rec_heads, -1)
    forget_pre = projected[1].astype(jnp.float32).reshape(height, rec_heads, -1)
    values = projected[2].astype(jnp.float32).reshape(height, rec_heads, -1)
    inflow = (1.0 - gate_floor.reshape(rec_heads, -1)) * jax.nn.sigmoid(-forget_pre)
    decays = jnp.log1p(-inflow) - extra_decay[:, :, None]
    local_out, final_state = local_recurrence(query_rows, decays, inflow, values)
    running_total = jnp.cumsum(decays, axis=0)
    overall = running_total[-1]

    def compose(earlier, latter):
        return (earlier[0] * latter[0], latter[0][..., None] * earlier[1] + latter[1])

    identity = (jnp.ones_like(overall), jnp.zeros_like(final_state))
    passed, arriving = prefix((jnp.exp(overall), final_state), "sp", compose, identity)
    incoming_rows = passed[..., None] * start_state + arriving
    carried_out = jnp.einsum(
        "dzc,zcu->dzu", query_rows * jnp.exp(running_total), incoming_rows, precision=TOP_PRECISION
    )
    rec_rows = head_norm(local_out + carried_out, recur_gain).astype(jnp.bfloat16)
    att_heads = gate_cache.shape[1]
    att_query = projected[3].reshape(height, att_heads, FD)
    offset = lax.axis_index("sp") * height
    scaling = FD ** (-0.5)
    groups = ((att_query, offset, height),)
    prepared = tuple(
        (
            (
                group_query,
                lax.dynamic_slice_in_dim(gate_cache, group_start, rows, 0),
                group_start + jnp.arange(rows),
            )
            for group_query, group_start, rows in groups
        )
    )
    initial = tuple(
        (
            (
                jnp.full((att_heads, rows), -1e30, jnp.float32),
                jnp.zeros((att_heads, rows), jnp.float32),
                jnp.zeros((rows, att_heads, FD), jnp.float32),
            )
            for _, _, rows in groups
        )
    )
    key_part = lax.all_gather(projected[4], "sp", axis=0, tiled=True)
    value_part = lax.all_gather(projected[5], "sp", axis=0, tiled=True)
    total_amount = key_part.shape[0]
    step_rows = 2 * height

    def advance_keys(number, states):
        begin_at = number * step_rows
        key_rows = lax.dynamic_slice_in_dim(key_part, begin_at, step_rows, 0).reshape(
            step_rows, att_heads, FD
        )
        value_rows = lax.dynamic_slice_in_dim(value_part, begin_at, step_rows, 0).reshape(
            step_rows, att_heads, FD
        )
        key_gates = lax.dynamic_slice_in_dim(gate_cache, begin_at, step_rows, 0)
        key_index = begin_at + jnp.arange(step_rows)
        updated = []
        for (group_query, group_gates, group_index), state in zip(prepared, states):
            compute = block_update(
                group_query,
                group_gates,
                group_index,
                key_rows,
                value_rows,
                key_gates,
                key_index,
                scaling,
            )
            needed = begin_at <= group_index[-1]
            updated.append(lax.cond(needed, compute, keep_state, state))
        return tuple(updated)

    folded = lax.fori_loop(0, total_amount // step_rows, advance_keys, initial)
    row_parts = [
        head_norm(summed / totals.T[:, :, None], attend_gain).astype(jnp.bfloat16)
        for maxima, totals, summed in folded
    ]
    att_rows = row_parts[0]
    rec_all, att_all = (
        lax.all_gather(rec_rows, "tp", axis=1, tiled=True),
        lax.all_gather(att_rows, "tp", axis=1, tiled=True),
    )
    layer_sum = jnp.dot(rec_all, recur_output, preferred_element_type=jnp.float32)
    layer_sum = layer_sum + jnp.dot(att_all, attend_output, preferred_element_type=jnp.float32)
    return layer_sum.astype(jnp.bfloat16)


def solution(mesh):
    return jax.shard_map(
        shards,
        mesh=mesh,
        in_specs=(
            P("sp", "tp"),
            P(),
            P(None, "tp"),
            P(None, "tp"),
            P(None, "tp"),
            P("tp"),
            P("sp", "tp"),
            P("tp", None, None),
            P("tp"),
            P(None, "tp"),
            P(None, "tp"),
            P(None, "tp"),
            P(None, "tp"),
            P("tp"),
            P(None, "tp"),
            P(None, "tp"),
        ),
        out_specs=P("sp", "tp"),
        check_vma=False,
    )
```

profile of v0, /device:TPU:31, one launch (start us, length us, event | category | flops | bytes accessed | tf_op | source)
XLA Modules:
  0.0 402.0 jit_solution(830316774274925419)
XLA Ops:
  8.8 10.7 %all-gather.6.cloned.1.call-done = bf16[256,2048]{1,0:T(8,128)(2,1)} async-done(((bf16[256,1024]{1,0:T(8,128)(2,1)}), bf16[256,2048]{1,0:T(8,128)(2,1)}) %all-gather.6.cloned.1.call-update) | async-done | bytes 1048592 | tf_op jit(solution)/shard_map/all_gather | solution.py:128
  33.8 76.5 %while.47 = (s32[]{:T(128)}, f32[4,128,128]{2,1,0:T(8,128)S(1)}, f32[4,64,4,128]{3,1,0,2:T(8,128)}, f32[4,64,4,128]{3,2,1,0:T(4,128)}, f32[4,64,4,128]{3,2,1,0:T...) while((s32[]{:T(128)}, f32[4,128,128]{2,1,0:T(8,128)S(1)}, ...), condition=%wide.region_3.4_spmd.clone, body=%wide.region_1.3_spmd.clone.sunk | while | flops 138760192 | bytes 21254276 | solution.py:68
  34.8 5.9 %exponential_bitcast_fusion.2 = f32[4,64,64,128]{3,0,2,1:T(4,128)S(1)} fusion(f32[64,4,128]{2,1,0:T(4,128)S(1)} %fusion.102, pred[64,64]{1,0:T(8,128)(4,1)S(1)} %fusion.104), kind=kLoop, calls=%fused_computation.29.clone.1 | loop fusion | flops 4194304 | bytes 8523776 | tf_op jit(solution)/shard_map/while
  41.6 7.3 %fusion.105 = f32[4,64,64]{1,2,0:T(8,128)S(1)} fusion(f32[4,64,64,128]{3,0,2,1:T(4,128)S(1)} %exponential_bitcast_fusion.2, f32[4,128,64]{1,2,0:T(8,128)S(1)} %copy.154, f32[4,128,64]{1,2,0:T(8,128)S(1)} %copy.155), kind=kLoop, calls=%fused_computation.28.clone.1 | loop fusion | flops 6275072 | bytes 8716288 | tf_op jit(solution)/shard_map/while/body/eval_jaxpr/thk,shk,tshk->hts/dot_general | solution.py:50
  53.9 5.9 %exponential_bitcast_fusion.2 = f32[4,64,64,128]{3,0,2,1:T(4,128)S(1)} fusion(f32[64,4,128]{2,1,0:T(4,128)S(1)} %fusion.102, pred[64,64]{1,0:T(8,128)(4,1)S(1)} %fusion.104), kind=kLoop, calls=%fused_computation.29.clone.1 | loop fusion | flops 4194304 | bytes 8523776 | tf_op jit(solution)/shard_map/while
  60.8 7.3 %fusion.105 = f32[4,64,64]{1,2,0:T(8,128)S(1)} fusion(f32[4,64,64,128]{3,0,2,1:T(4,128)S(1)} %exponential_bitcast_fusion.2, f32[4,128,64]{1,2,0:T(8,128)S(1)} %copy.154, f32[4,128,64]{1,2,0:T(8,128)S(1)} %copy.155), kind=kLoop, calls=%fused_computation.28.clone.1 | loop fusion | flops 6275072 | bytes 8716288 | tf_op jit(solution)/shard_map/while/body/eval_jaxpr/thk,shk,tshk->hts/dot_general | solution.py:50
  79.9 7.3 %fusion.105 = f32[4,64,64]{1,2,0:T(8,128)S(1)} fusion(f32[4,64,64,128]{3,0,2,1:T(4,128)S(1)} %exponential_bitcast_fusion.2, f32[4,128,64]{1,2,0:T(8,128)S(1)} %copy.154, f32[4,128,64]{1,2,0:T(8,128)S(1)} %copy.155), kind=kLoop, calls=%fused_computation.28.clone.1 | loop fusion | flops 6275072 | bytes 8716288 | tf_op jit(solution)/shard_map/while/body/eval_jaxpr/thk,shk,tshk->hts/dot_general | solution.py:50
  99.0 7.3 %fusion.105 = f32[4,64,64]{1,2,0:T(8,128)S(1)} fusion(f32[4,64,64,128]{3,0,2,1:T(4,128)S(1)} %exponential_bitcast_fusion.2, f32[4,128,64]{1,2,0:T(8,128)S(1)} %copy.154, f32[4,128,64]{1,2,0:T(8,128)S(1)} %copy.155), kind=kLoop, calls=%fused_computation.28.clone.1 | loop fusion | flops 6275072 | bytes 8716288 | tf_op jit(solution)/shard_map/while/body/eval_jaxpr/thk,shk,tshk->hts/dot_general | solution.py:50
  124.4 28.4 %all_gather.26 = bf16[16,4,128]{2,1,0:T(4,128)(2,1)S(1)} all-gather(bf16[1,4,128]{2,1,0:T(4,128)(2,1)S(1)} %fusion.69), channel_id=1, replica_groups=mesh['sp'=16,'tp'=2] {'sp'}, dimensions={0}, use_global_device_ids=true | all-gather | bytes 17408 | tf_op jit(solution)/shard_map/all_gather | solution.py:16
  158.0 10.9 %all-gather.12.cloned.1.call-done = bf16[64,128,128]{2,1,0:T(8,128)(2,1)} async-done(((bf16[4,128,128]{2,1,0:T(8,128)(2,1)}), bf16[64,128,128]{2,1,0:T(8,128)(2,1)}) %all-gather.12.cloned.1.call-update) | async-done | bytes 2097168 | tf_op jit(solution)/shard_map/all_gather | solution.py:16
  168.9 18.7 %while.48 = (s32[]{:T(128)}, f32[4,128]{1,0:T(4,128)S(1)}, f32[4,128,128]{2,1,0:T(8,128)S(1)}, s32[]{:T(128)}, bf16[16,4,128]{2,1,0:T(4,128)(2,1)S(1)}, /*index=...) while((s32[]{:T(128)}, f32[4,128]{1,0:T(4,128)S(1)}, f32[4,128,128]{2,1,0:T(8,128)S(1)}, ...), condition=%wide.region_7.8_spmd.clone, body=%wide.region_6.7_spmd.clone.sunk | while | flops 330244 | bytes 665727 | solution.py:29
  193.8 52.4 %all-gather.8.cloned.1.call-done = bf16[4096,512]{1,0:T(8,128)(2,1)} async-done(((bf16[256,512]{1,0:T(8,128)(2,1)}), bf16[4096,512]{1,0:T(8,128)(2,1)}) %all-gather.8.cloned.1.call-update) | async-done | bytes 4194320 | tf_op jit(solution)/shard_map/all_gather | solution.py:184
  246.2 6.4 %copy.101 = bf16[4096,512]{0,1:T(8,128)(2,1)} copy(bf16[4096,512]{1,0:T(8,128)(2,1)} %all-gather.8.cloned.1.call-done) | data formatting | bytes 8388608 | tf_op jit(solution)/shard_map/while | solution.py:215
  252.6 70.5 %all-gather.10.cloned.1.call-done = bf16[4096,512]{1,0:T(8,128)(2,1)} async-done(((bf16[256,512]{1,0:T(8,128)(2,1)}), bf16[4096,512]{1,0:T(8,128)(2,1)}) %all-gather.10.cloned.1.call-update) | async-done | bytes 4194320 | tf_op jit(solution)/shard_map/all_gather | solution.py:185
  323.0 6.4 %copy.102 = bf16[4096,512]{0,1:T(8,128)(2,1)} copy(bf16[4096,512]{1,0:T(8,128)(2,1)} %all-gather.10.cloned.1.call-done) | data formatting | bytes 8388608 | tf_op jit(solution)/shard_map/while | solution.py:215
  329.5 60.8 %while.46 = (s32[]{:T(128)}, f32[8,256]{1,0:T(8,128)S(1)}, f32[8,256]{1,0:T(8,128)S(1)}, f32[256,8,64]{0,2,1:T(8,128)S(1)}, s32[256]{0:T(256)S(1)}, /*index=5*/b...) while((s32[]{:T(128)}, f32[8,256]{1,0:T(8,128)S(1)}, ...), condition=%wide.region_14.15_spmd, body=%wide.region_9.14_spmd.sunk | while | flops 286661120 | bytes 17810780 | solution.py:215
  330.7 6.3 %conditional.2 = ((f32[8,256]{1,0:T(8,128)S(1)}, f32[8,256]{1,0:T(8,128)S(1)}, f32[256,8,64]{0,2,1:T(8,128)S(1)})) conditional(s32[]{:T(128)} %convert_element_type.161, (f32[8,256]{1,0:T(8,128)S(1)}, f32[8,256]{1,0:T(8,128)S(1)}, f32[256,8,64]{0,2,1:T(8,128)S(1)}) %tuple.108, (s32[]{:T(128)}, s32[512]{0:T(512)S(1)}, s32[256]{0:T(256)S(1)}, ...), branch_computations={%region_10.10_spmd, %region_11.13_spmd} | conditional | flops 286661120 | bytes 17808462 | solution.py:212
  338.3 6.3 %conditional.2 = ((f32[8,256]{1,0:T(8,128)S(1)}, f32[8,256]{1,0:T(8,128)S(1)}, f32[256,8,64]{0,2,1:T(8,128)S(1)})) conditional(s32[]{:T(128)} %convert_element_type.161, (f32[8,256]{1,0:T(8,128)S(1)}, f32[8,256]{1,0:T(8,128)S(1)}, f32[256,8,64]{0,2,1:T(8,128)S(1)}) %tuple.108, (s32[]{:T(128)}, s32[512]{0:T(512)S(1)}, s32[256]{0:T(256)S(1)}, ...), branch_computations={%region_10.10_spmd, %region_11.13_spmd} | conditional | flops 286661120 | bytes 17808462 | solution.py:212
  345.9 6.3 %conditional.2 = ((f32[8,256]{1,0:T(8,128)S(1)}, f32[8,256]{1,0:T(8,128)S(1)}, f32[256,8,64]{0,2,1:T(8,128)S(1)})) conditional(s32[]{:T(128)} %convert_element_type.161, (f32[8,256]{1,0:T(8,128)S(1)}, f32[8,256]{1,0:T(8,128)S(1)}, f32[256,8,64]{0,2,1:T(8,128)S(1)}) %tuple.108, (s32[]{:T(128)}, s32[512]{0:T(512)S(1)}, s32[256]{0:T(256)S(1)}, ...), branch_computations={%region_10.10_spmd, %region_11.13_spmd} | conditional | flops 286661120 | bytes 17808462 | solution.py:212
  353.5 6.3 %conditional.2 = ((f32[8,256]{1,0:T(8,128)S(1)}, f32[8,256]{1,0:T(8,128)S(1)}, f32[256,8,64]{0,2,1:T(8,128)S(1)})) conditional(s32[]{:T(128)} %convert_element_type.161, (f32[8,256]{1,0:T(8,128)S(1)}, f32[8,256]{1,0:T(8,128)S(1)}, f32[256,8,64]{0,2,1:T(8,128)S(1)}) %tuple.108, (s32[]{:T(128)}, s32[512]{0:T(512)S(1)}, s32[256]{0:T(256)S(1)}, ...), branch_computations={%region_10.10_spmd, %region_11.13_spmd} | conditional | flops 286661120 | bytes 17808462 | solution.py:212
  361.1 6.3 %conditional.2 = ((f32[8,256]{1,0:T(8,128)S(1)}, f32[8,256]{1,0:T(8,128)S(1)}, f32[256,8,64]{0,2,1:T(8,128)S(1)})) conditional(s32[]{:T(128)} %convert_element_type.161, (f32[8,256]{1,0:T(8,128)S(1)}, f32[8,256]{1,0:T(8,128)S(1)}, f32[256,8,64]{0,2,1:T(8,128)S(1)}) %tuple.108, (s32[]{:T(128)}, s32[512]{0:T(512)S(1)}, s32[256]{0:T(256)S(1)}, ...), branch_computations={%region_10.10_spmd, %region_11.13_spmd} | conditional | flops 286661120 | bytes 17808462 | solution.py:212
  368.7 6.3 %conditional.2 = ((f32[8,256]{1,0:T(8,128)S(1)}, f32[8,256]{1,0:T(8,128)S(1)}, f32[256,8,64]{0,2,1:T(8,128)S(1)})) conditional(s32[]{:T(128)} %convert_element_type.161, (f32[8,256]{1,0:T(8,128)S(1)}, f32[8,256]{1,0:T(8,128)S(1)}, f32[256,8,64]{0,2,1:T(8,128)S(1)}) %tuple.108, (s32[]{:T(128)}, s32[512]{0:T(512)S(1)}, s32[256]{0:T(256)S(1)}, ...), branch_computations={%region_10.10_spmd, %region_11.13_spmd} | conditional | flops 286661120 | bytes 17808462 | solution.py:212
  376.3 6.3 %conditional.2 = ((f32[8,256]{1,0:T(8,128)S(1)}, f32[8,256]{1,0:T(8,128)S(1)}, f32[256,8,64]{0,2,1:T(8,128)S(1)})) conditional(s32[]{:T(128)} %convert_element_type.161, (f32[8,256]{1,0:T(8,128)S(1)}, f32[8,256]{1,0:T(8,128)S(1)}, f32[256,8,64]{0,2,1:T(8,128)S(1)}) %tuple.108, (s32[]{:T(128)}, s32[512]{0:T(512)S(1)}, s32[256]{0:T(256)S(1)}, ...), branch_computations={%region_10.10_spmd, %region_11.13_spmd} | conditional | flops 286661120 | bytes 17808462 | solution.py:212
  383.9 6.3 %conditional.2 = ((f32[8,256]{1,0:T(8,128)S(1)}, f32[8,256]{1,0:T(8,128)S(1)}, f32[256,8,64]{0,2,1:T(8,128)S(1)})) conditional(s32[]{:T(128)} %convert_element_type.161, (f32[8,256]{1,0:T(8,128)S(1)}, f32[8,256]{1,0:T(8,128)S(1)}, f32[256,8,64]{0,2,1:T(8,128)S(1)}) %tuple.108, (s32[]{:T(128)}, s32[512]{0:T(512)S(1)}, s32[256]{0:T(256)S(1)}, ...), branch_computations={%region_10.10_spmd, %region_11.13_spmd} | conditional | flops 286661120 | bytes 17808462 | solution.py:212
  (281 shorter events, 155.2 us)
Async XLA Ops:
  6.5 186.6 %copy-start = (bf16[1024,1024]{1,0:T(8,128)(2,1)S(1)}, bf16[1024,1024]{1,0:T(8,128)(2,1)}, u32[]{:S(2)}) copy-start(bf16[1024,1024]{1,0:T(8,128)(2,1)} %param.38) | copy-start | bytes 6291460
  6.5 13.0 %all-gather.6.cloned.1.call-start = ((), (), s32[]{:S(2)}) async-start(), calls=%async_computation | async-start | bytes 1572864 | tf_op jit(solution)/shard_map/all_gather | solution.py:128
  7.3 161.7 %all-gather.12.cloned.1.call-start = ((), (), s32[]{:S(2)}) async-start(), calls=%async_computation.3 | async-start | bytes 2228224 | tf_op jit(solution)/shard_map/all_gather | solution.py:16
  21.1 3.8 copy-start.14
  23.8 3.6 copy-start.4
  31.1 2.7 copy-start.6
  111.0 4.5 %copy-start.7 = (f32[256,512]{1,0:T(8,128)S(1)}, f32[256,512]{1,0:T(8,128)}, u32[]{:S(2)}) copy-start(f32[256,512]{1,0:T(8,128)} %copy-done.6) | copy-start | bytes 1572868
  111.0 135.2 %all-gather.8.cloned.1.call-start = ((), (), s32[]{:S(2)}) async-start(), calls=%async_computation.1 | async-start | bytes 4456448 | tf_op jit(solution)/shard_map/all_gather | solution.py:184
  114.5 4.1 %copy-start.5 = (f32[256,512]{1,0:T(8,128)S(1)}, f32[256,512]{1,0:T(8,128)}, u32[]{:S(2)}) copy-start(f32[256,512]{1,0:T(8,128)} %copy-done.4) | copy-start | bytes 1572868
  114.5 4.1 %copy-start.10 = (f32[256,4]{0,1:T(4,128)S(1)}, f32[256,4]{0,1:T(4,128)}, u32[]{:S(2)}) copy-start(f32[256,4]{0,1:T(4,128)} %param.30) | copy-start | bytes 12292
  114.5 208.5 %all-gather.10.cloned.1.call-start = ((), (), s32[]{:S(2)}) async-start(), calls=%async_computation.2 | async-start | bytes 4456448 | tf_op jit(solution)/shard_map/all_gather | solution.py:185
  119.2 1.2 copy-start.8
  119.2 2.0 copy-start.13
  158.0 29.7 %copy-start.2 = (f32[256,4,128]{0,2,1:T(8,128)S(1)}, f32[256,4,128]{0,2,1:T(8,128)}, u32[]{:S(2)}) copy-start(f32[256,4,128]{0,2,1:T(8,128)} %copy.99) | copy-start | bytes 1572868
  187.7 1.8 copy-start.11
  252.6 76.9 %copy-start.9 = (bf16[256,512]{0,1:T(8,128)(2,1)S(1)}, bf16[256,512]{0,1:T(8,128)(2,1)}, u32[]{:S(2)}) copy-start(bf16[256,512]{0,1:T(8,128)(2,1)} %copy.100) | copy-start | bytes 786436
  329.5 61.0 %copy-start.12 = (f32[512]{0:T(512)S(1)}, f32[512]{0:T(512)}, u32[]{:S(2)}) copy-start(f32[512]{0:T(512)} %param.37) | copy-start | bytes 6148
  390.3 3.7 copy-start.3
  390.6 4.9 %copy-start.1 = (bf16[1024,1024]{1,0:T(8,128)(2,1)S(1)}, bf16[1024,1024]{1,0:T(8,128)(2,1)}, u32[]{:S(2)}) copy-start(bf16[1024,1024]{1,0:T(8,128)(2,1)} %param.38) | copy-start | bytes 6291460
Sparse Core Ops, SparseCore 0:
  8.9 10.6 all-gather.5
  111.1 57.7 all-gather.11
  171.7 74.4 all-gather.7
  248.8 74.1 all-gather.9
where the time goes:
time: 405 us; the launch traced here: 402 us
  waiting for transfers between devices  145 us (36%)
  other arithmetic  99 us (24%)
  local copies, waits for them, and re-layouts  51.6 us (13%)
  matrix products  50.3 us (12%)
  blocking collectives  35.3 us (9%)
  between operations  13.5 us (3%)
  loops' own time  6.83 us (2%)
    all_gather x1, waiting for transfers between devices, shards(): value_part = lax.all_gather(projected[5], 'sp', axis=0, tiled=True)  70.5 us
    all_gather x1, waiting for transfers between devices, shards(): key_part = lax.all_gather(projected[4], 'sp', axis=0, tiled=True)  52.4 us
    dot_general x4, other arithmetic, advance(): jnp.einsum('thk,shk,tshk->hts', query_block, k_block, jnp.exp(offsets), p...  29.1 us
    all_gather x1, blocking collectives, prefix(): lax.all_gather(part.astype(kind), axis)  28.4 us
    while x4, other arithmetic  23.5 us
    select_n x32, other arithmetic, step(): return jax.tree.map(lambda a, b: jnp.where(reached, a, b), new, before)  17.9 us
    dot_general x6, matrix products, shards(): jnp.dot(scaled, weight, preferred_element_type=jnp.float32)  16.4 us
    while x2, local copies, waits for them, and re-layouts, shards(): folded = lax.fori_loop(0, total_amount // step_rows, advance_keys, initial)  12.8 us
  transfers between devices with their start and end apart: 4, of which 4 were waited for; matrix products, arithmetic and copies ran while one was open for 11% of the time, Pallas kernels for 0%

commit v1 on v0

v1 whole, which is shorter than its diff:
```python
import functools
import math

import jax
import jax.numpy as jnp
from jax import lax
from jax.experimental import pallas as pl
from jax.experimental.pallas import tpu as pltpu
from jax.sharding import PartitionSpec as P

FD = 64
KD = 128
EPSILON = 1e-06
BLOCK = 32
MESH = pl.DeviceIdType.MESH
F32 = jnp.float32
BF16 = jnp.bfloat16


def dot(a, b, ca=1, cb=0):
    return lax.dot_general(a, b, (((ca,), (cb,)), ((), ())), preferred_element_type=F32)


def layer_kernel(
    dims,
    tokens, gain, gate_floor, extra_decay, start_state, recur_gain, gates, attend_gain,
    w_ak, w_av, w_aq, w_rq, w_rf, w_rv, w_ro, w_ao,
    out,
    wbuf, wout, tok_all, scaled, proj, kv_all, q_all, m_ref, l_ref, acc, part, part_l,
    comb, comb_l, cum_ref, qe, rec_o, mix, st_all, chain_out, chain_in, rows_all,
    w_sem, wo_sem, tok_s, tok_r, q_s, q_r, st_s, st_r, kv_s, kv_r, ch_s, ch_r,
    po_s, po_r, pl_s, pl_r, rr_s, rr_r, ra_s, ra_r,
):
    Z, G, TP = dims
    rows, width = tokens.shape[0], recur_gain.shape[1]
    part_w = tokens.shape[1]
    model = part_w * TP
    rec_heads, att_heads = width // KD, width // FD
    c, t = lax.axis_index("sp"), lax.axis_index("tp")
    z, i = c // G, c % G

    loads = [
        pltpu.make_async_copy(w, wbuf.at[k], w_sem.at[k])
        for k, w in enumerate((w_ak, w_av, w_aq, w_rq, w_rf, w_rv))
    ]
    out_loads = [
        pltpu.make_async_copy(w, wout.at[k], wo_sem.at[k]) for k, w in enumerate((w_ro, w_ao))
    ]
    for load in loads + out_loads:
        load.start()

    barrier = pltpu.get_barrier_semaphore()
    tp_peers = [(c, (t + d) % TP) for d in range(1, TP)]
    inner_peers = [(z * G + (i + d) % G, t) for d in range(1, G)]
    outer_peers = [(((z + d) % Z) * G + i, t) for d in range(1, Z)]
    for peer in tp_peers + inner_peers + outer_peers:
        pl.semaphore_signal(barrier, inc=1, device_id=peer, device_id_type=MESH)
    pl.semaphore_wait(barrier, TP - 1 + G - 1 + Z - 1)

    def remote(src, dst, s, r, peer):
        return pltpu.make_async_remote_copy(
            src_ref=src, dst_ref=dst, send_sem=s, recv_sem=r, device_id=peer, device_id_type=MESH
        )

    tok_copies = [
        remote(tokens, tok_all.at[t], tok_s.at[d], tok_r.at[d], peer)
        for d, peer in enumerate(tp_peers)
    ]
    for copy in tok_copies:
        copy.start()
    tok_all[t] = tokens[...]
    for copy in tok_copies:
        copy.wait_recv()
    squares = jnp.zeros((rows, 1), F32)
    for p in range(TP):
        x = tok_all[p].astype(F32)
        squares = squares + jnp.sum(x * x, axis=1, keepdims=True)
        scaled[:, p * part_w:(p + 1) * part_w] = (x * gain[p]).astype(BF16)
    inverse = lax.rsqrt(squares / model + EPSILON)

    def project(k):
        return dot(scaled[...], wbuf[k]) * inverse

    loads[0].wait()
    loads[1].wait()

    def project_kv(k, carry):
        kv_all[z, k] = project(k).T.astype(BF16)
        return carry

    lax.fori_loop(0, 2, project_kv, 0)

    def kv_copy(slot):
        return remote(
            kv_all.at[slot], kv_all.at[slot], kv_s.at[slot], kv_r.at[slot], (c + G, t)
        )

    last = z == Z - 1

    @pl.when(jnp.logical_not(last))
    def _():
        kv_copy(z).start()

    loads[2].wait()
    q_all[i] = (project(2) * FD ** (-0.5)).T.astype(BF16)
    q_copies = [
        remote(q_all.at[i], q_all.at[i], q_s.at[d], q_r.at[d], peer)
        for d, peer in enumerate(inner_peers)
    ]
    for copy in q_copies:
        copy.start()
    for k in range(3, 6):
        loads[k].wait()

    def project_rec(k, carry):
        proj[k - 3] = project(k).astype(BF16)
        return carry

    lax.fori_loop(3, 6, project_rec, 0)

    rows_i = lax.broadcasted_iota(jnp.int32, (rows, rows), 0)
    cols_i = lax.broadcasted_iota(jnp.int32, (rows, rows), 1)
    lower = (cols_i <= rows_i).astype(F32).astype(BF16)
    for h in range(rec_heads):
        lanes = slice(h * KD, (h + 1) * KD)
        query = proj[0, :, lanes].astype(F32)
        value = proj[2, :, lanes]
        inflow = (1.0 - gate_floor[:, lanes]) * jax.nn.sigmoid(-proj[1, :, lanes].astype(F32))
        decay = jnp.log1p(-inflow) - extra_decay[:, h:h + 1]
        high = decay.astype(BF16)
        rest = decay - high.astype(F32)
        mid = rest.astype(BF16)
        low = (rest - mid.astype(F32)).astype(BF16)
        cum_ref[...] = dot(lower, high) + (dot(lower, mid) + dot(lower, low))
        cum = cum_ref[...]
        qe[:, lanes] = (query * jnp.exp(cum)).astype(BF16)
        end = cum[rows - 1:rows]
        key_end = (inflow * jnp.exp(end - cum)).astype(BF16)
        st_all[i, h, :KD] = dot(value, key_end, 0, 0).astype(BF16)
        st_all[i, h, KD:] = jnp.broadcast_to(jnp.exp(end), (16, KD)).astype(BF16)
        mix[...] = jnp.zeros_like(mix)
        for b in range(rows // BLOCK):
            low_r, high_r = b * BLOCK, (b + 1) * BLOCK
            middle = cum[low_r + BLOCK // 2 - 1:low_r + BLOCK // 2]
            qb = (query[low_r:high_r] * jnp.exp(cum[low_r:high_r] - middle)).astype(BF16)
            kb = (inflow[:high_r] * jnp.exp(middle - cum[:high_r])).astype(BF16)
            a = dot(qb, kb, 1, 1)
            row_at = low_r + lax.broadcasted_iota(jnp.int32, a.shape, 0)
            col_at = lax.broadcasted_iota(jnp.int32, a.shape, 1)
            mix[low_r:high_r, :high_r] = jnp.where(col_at <= row_at, a, 0.0)
        rec_o[:, lanes] = dot(mix[...].astype(BF16), value)

    st_copies = [
        remote(st_all.at[i], st_all.at[i], st_s.at[d], st_r.at[d], peer)
        for d, peer in enumerate(inner_peers)
    ]
    for copy in st_copies:
        copy.start()

    m_ref[...] = jnp.full_like(m_ref, -1e30)
    l_ref[...] = jnp.zeros_like(l_ref)
    acc[...] = jnp.zeros_like(acc)
    for copy in q_copies:
        copy.wait_recv()

    def attend(slot, j, diagonal):
        key_gates = gates[pl.ds(pl.multiple_of((slot * G + i) * rows, rows), rows), :]
        first = gates[pl.ds(pl.multiple_of((z * G + j) * rows, rows), 1), :]
        bias = first - key_gates
        if diagonal:
            allowed = i * rows + rows_i <= j * rows + cols_i
        for h in range(att_heads):
            span = slice(h * FD, (h + 1) * FD)
            s = dot(kv_all[slot, 0, span, :], q_all[j, span, :], 0, 0) + bias[:, h:h + 1]
            if diagonal:
                s = jnp.where(allowed, s, -1e30)
            before = m_ref[j, h:h + 1, :]
            top = jnp.maximum(before, jnp.max(s, axis=0, keepdims=True))
            w = jnp.exp(s - top)
            fade = jnp.exp(before - top)
            m_ref[j, h:h + 1, :] = top
            l_ref[j, h:h + 1, :] = l_ref[j, h:h + 1, :] * fade + jnp.sum(w, axis=0, keepdims=True)
            acc[j, span, :] = acc[j, span, :] * fade + dot(kv_all[slot, 1, span, :], w.astype(BF16))

    def part_copies(d):
        j = (i + d) % G
        peer = (z * G + j, t)
        return (
            remote(part.at[j], comb.at[i], po_s.at[d], po_r.at[d], peer),
            remote(part_l.at[j], comb_l.at[i], pl_s.at[d], pl_r.at[d], peer),
        )

    def finish(d):
        j = (i + d) % G
        total = jnp.maximum(l_ref[j], 1e-30)
        part_l[j] = m_ref[j] + jnp.log(total)
        for h in range(att_heads):
            span = slice(h * FD, (h + 1) * FD)
            part[j, span, :] = (acc[j, span, :] / total[h:h + 1]).astype(BF16)

        @pl.when(d < G)
        def _():
            for copy in part_copies(d):
                copy.start()

    def own_slot(d, carry):
        j = (i + d) % G

        @pl.when(j >= i)
        def _():
            attend(z, j, True)

        @pl.when(z == 0)
        def _():
            finish(d)

        return carry

    lax.fori_loop(1, G + 1, own_slot, 0)

    def earlier_slot(n, carry):
        slot = z - n
        kv_copy(slot).wait_recv()

        @pl.when(jnp.logical_not(last))
        def _():
            kv_copy(slot).start()

        def one(d, inner):
            attend(slot, (i + d) % G, False)

            @pl.when(slot == 0)
            def _():
                finish(d)

            return inner

        lax.fori_loop(1, G + 1, one, 0)
        return carry

    lax.fori_loop(1, z + 1, earlier_slot, 0)

    for copy in st_copies:
        copy.wait_recv()
    chain_copy = remote(chain_out, chain_in, ch_s, ch_r, (c + G, t))

    @pl.when(z == 0)
    def _():
        for h in range(rec_heads):
            chain_in[h] = start_state[h].T.astype(BF16)

    @pl.when(z > 0)
    def _():
        chain_copy.wait_recv()

    for h in range(rec_heads):
        lanes = slice(h * KD, (h + 1) * KD)

        def pass_on(k, state):
            return st_all[k, h, KD:KD + 1].astype(F32) * state + st_all[k, h, :KD].astype(F32)

        state = lax.fori_loop(0, i, pass_on, chain_in[h].astype(F32))
        chain_out[h] = lax.fori_loop(i, G, pass_on, state).astype(BF16)
        rec_o[:, lanes] = rec_o[:, lanes] + dot(qe[:, lanes], state.astype(BF16), 1, 1)

    @pl.when(jnp.logical_not(last))
    def _():
        chain_copy.start()

    for h in range(rec_heads):
        lanes = slice(h * KD, (h + 1) * KD)
        x = rec_o[:, lanes]
        x = x * lax.rsqrt(jnp.mean(x * x, axis=1, keepdims=True) + EPSILON)
        rows_all[0, t, :, lanes] = (x * recur_gain[:, lanes]).astype(BF16)
    row_copies = [
        [
            remote(rows_all.at[k, t], rows_all.at[k, t], s.at[d], r.at[d], peer)
            for d, peer in enumerate(tp_peers)
        ]
        for k, (s, r) in enumerate(((rr_s, rr_r), (ra_s, ra_r)))
    ]
    for copy in row_copies[0]:
        copy.start()

    comb[i] = part[i]
    comb_l[i] = part_l[i]
    for d in range(1, G):
        for copy in part_copies(d):
            copy.wait_recv()
    top = comb_l[0]
    for k in range(1, G):
        top = jnp.maximum(top, comb_l[k])
    shares = [jnp.exp(comb_l[k] - top) for k in range(G)]
    whole = shares[0]
    for k in range(1, G):
        whole = whole + shares[k]
    for h in range(att_heads):
        span = slice(h * FD, (h + 1) * FD)
        x = jnp.zeros((FD, rows), F32)
        for k in range(G):
            x = x + comb[k, span, :].astype(F32) * (shares[k][h:h + 1] / whole[h:h + 1])
        acc[0, span, :] = x * lax.rsqrt(jnp.mean(x * x, axis=0, keepdims=True) + EPSILON)
    rows_all[1, t] = (acc[0].T * attend_gain[...]).astype(BF16)
    for copy in row_copies[1]:
        copy.start()

    for load in out_loads:
        load.wait()
    for copy in row_copies[0] + row_copies[1]:
        copy.wait_recv()
    tile = min(256, out.shape[1])

    def output(n, carry):
        columns = pl.ds(pl.multiple_of(n * tile, tile), tile)
        total = jnp.zeros((rows, tile), F32)
        for k in range(2):
            for p in range(TP):
                total = total + dot(rows_all[k, p], wout[k, p * width:(p + 1) * width, columns])
        out[:, columns] = total.astype(BF16)
        return carry

    lax.fori_loop(0, out.shape[1] // tile, output, 0)

    for copy in tok_copies + q_copies + st_copies + row_copies[0] + row_copies[1]:
        copy.wait_send()
    for d in range(1, G):
        for copy in part_copies(d):
            copy.wait_send()

    @pl.when(jnp.logical_not(last))
    def _():
        chain_copy.wait_send()

        def sent(n, carry):
            kv_copy(z - n).wait_send()
            return carry

        lax.fori_loop(0, z + 1, sent, 0)


def shards(
    sizes, tokens, norm_gain, recur_query, recur_forget, recur_value, gate_floor, extra_decay,
    start_state, recur_gain, attend_query, attend_key, attend_value, gate_cache, attend_gain,
    recur_output, attend_output,
):
    sp, TP = sizes
    G = math.isqrt(sp)
    while sp % G:
        G -= 1
    Z = sp // G
    rows, part_w = tokens.shape
    width = recur_gain.shape[0]
    model = norm_gain.shape[0]
    rec_heads, att_heads = width // KD, width // FD
    out_w = recur_output.shape[1]
    vmem = pl.BlockSpec(memory_space=pltpu.VMEM)
    anywhere = pl.BlockSpec(memory_space=pl.ANY)
    dma = pltpu.SemaphoreType.DMA
    return pl.pallas_call(
        functools.partial(layer_kernel, (Z, G, TP)),
        out_shape=jax.ShapeDtypeStruct((rows, out_w), BF16),
        in_specs=[vmem] * 8 + [anywhere] * 8,
        out_specs=vmem,
        scratch_shapes=[
            pltpu.VMEM((6, model, width), BF16),
            pltpu.VMEM((2, width * TP, out_w), BF16),
            pltpu.VMEM((TP, rows, part_w), BF16),
            pltpu.VMEM((rows, model), BF16),
            pltpu.VMEM((3, rows, width), BF16),
            pltpu.VMEM((Z, 2, width, rows), BF16),
            pltpu.VMEM((G, width, rows), BF16),
            pltpu.VMEM((G, att_heads, rows), F32),
            pltpu.VMEM((G, att_heads, rows), F32),
            pltpu.VMEM((G, width, rows), F32),
            pltpu.VMEM((G, width, rows), BF16),
            pltpu.VMEM((G, att_heads, rows), F32),
            pltpu.VMEM((G, width, rows), BF16),
            pltpu.VMEM((G, att_heads, rows), F32),
            pltpu.VMEM((rows, KD), F32),
            pltpu.VMEM((rows, width), BF16),
            pltpu.VMEM((rows, width), F32),
            pltpu.VMEM((rows, rows), F32),
            pltpu.VMEM((G, rec_heads, KD + 16, KD), BF16),
            pltpu.VMEM((rec_heads, KD, KD), BF16),
            pltpu.VMEM((rec_heads, KD, KD), BF16),
            pltpu.VMEM((2, TP, rows, width), BF16),
            dma((6,)), dma((2,)),
            dma((TP,)), dma((TP,)),
            dma((G,)), dma((G,)), dma((G,)), dma((G,)),
            dma((Z,)), dma((Z,)), dma, dma,
            dma((G,)), dma((G,)), dma((G,)), dma((G,)),
            dma((TP,)), dma((TP,)), dma((TP,)), dma((TP,)),
        ],
        compiler_params=pltpu.CompilerParams(
            collective_id=0, has_side_effects=True, vmem_limit_bytes=56 * 1024 * 1024
        ),
    )(
        tokens, norm_gain.reshape(TP, 1, part_w), gate_floor.reshape(1, width), extra_decay,
        start_state, recur_gain.reshape(1, width), gate_cache, attend_gain.reshape(1, width),
        attend_key, attend_value, attend_query, recur_query, recur_forget, recur_value,
        recur_output, attend_output,
    )


def solution(mesh):
    sizes = (mesh.shape["sp"], mesh.shape["tp"])
    return jax.shard_map(
        functools.partial(shards, sizes),
        mesh=mesh,
        in_specs=(
            P("sp", "tp"),
            P(),
            P(None, "tp"),
            P(None, "tp"),
            P(None, "tp"),
            P("tp"),
            P("sp", "tp"),
            P("tp", None, None),
            P("tp"),
            P(None, "tp"),
            P(None, "tp"),
            P(None, "tp"),
            P(None, "tp"),
            P("tp"),
            P(None, "tp"),
            P(None, "tp"),
        ),
        out_specs=P("sp", "tp"),
        check_vma=False,
    )
```

time: 405 us -> 83.8 us (0.21)
  waiting for transfers between devices: 145 us -> 0 us
  other arithmetic: 99 us -> 0 us
  Pallas kernels: 0 us -> 77.3 us
  matrix products: 50.3 us -> 0 us
  local copies, waits for them, and re-layouts: 51.6 us -> 6.21 us
  blocking collectives: 35.3 us -> 0 us
  between operations: 13.5 us -> 0.01 us
  loops' own time: 6.83 us -> 0 us
    all_gather x4 -> x0, waiting for transfers between devices: 144 us -> none  [the longest x1 70.5 us: shards(): value_part = lax.all_gather(projected[5], 'sp', axis=0, tiled=True)]
    pallas_call x0 -> x1, Pallas kernels: none -> 77.3 us  [shards(): pl.pallas_call(functools.partial(layer_kernel, (Z, G, TP)), out_shape=jax...]
    dot_general x37 -> x0, matrix products: 50.3 us -> none  [the longest x6 16.4 us: shards(): jnp.dot(scaled, weight, preferred_element_type=jnp.float32)]
    all_gather x3 -> x0, blocking collectives: 35.3 us -> none  [the longest x1 28.4 us: prefix(): lax.all_gather(part.astype(kind), axis)]
    dot_general x4 -> x0, other arithmetic: 29.1 us -> none  [advance(): jnp.einsum('thk,shk,tshk->hts', query_block, k_block, jnp.exp(offsets), p...]
    while x4 -> x0, other arithmetic: 23.5 us -> none
    select_n x32 -> x0, other arithmetic: 17.9 us -> none  [step(): return jax.tree.map(lambda a, b: jnp.where(reached, a, b), new, before)]
    dynamic_slice x13 -> x0, local copies, waits for them, and re-layouts: 14.6 us -> none  [the longest x8 10.2 us: advance_keys(): lax.dynamic_slice_in_dim(value_part, begin_at, step_rows, 0)]
  transfers between devices with their start and end apart: 4 -> 0, of which waited for: 4 -> 0; matrix products, arithmetic and copies ran while one was open for 11% -> 0% of each run, Pallas kernels for 0% -> 0%
where the time goes in v1:
time: 83.8 us; the launch traced here: 83.5 us
  Pallas kernels  77.3 us (92%)
  local copies, waits for them, and re-layouts  6.21 us (7%)
    pallas_call x1, Pallas kernels, shards(): pl.pallas_call(functools.partial(layer_kernel, (Z, G, TP)), out_shape=jax...  77.3 us
    unnamed x3, local copies, waits for them, and re-layouts  6.21 us

profile of v1, /device:TPU:31, one launch (start us, length us, event | category | flops | bytes accessed | tf_op | source)
XLA Modules:
  0.0 83.5 jit_solution(322764629209396171)
XLA Ops:
  0.0 1.5 %copy.17.extra_decay = f32[256,4]{1,0:T(8,128)} copy(f32[256,4]{0,1:T(4,128)} %param.22) | data formatting | bytes 8192 | tf_op args[6]
  1.5 2.9 %copy.18.gates = f32[4096,8]{1,0:T(8,128)} copy(f32[4096,8]{0,1:T(8,128)} %param.28) | data formatting | bytes 262144 | tf_op args[12]
  4.3 77.3 %shard_map.154 = bf16[256,1024]{1,0:T(8,128)(2,1)} custom-call(bf16[256,1024]{1,0:T(8,128)(2,1)} %tokens.1, f32[2,1,1024]{2,1,0:T(1,128)} %bitcast.4, f32[1,512]{1,0:T(1,128)} %bitcast.5, f32[256,4]{1,0:T(8,128)} %copy.17.extra_decay, f32[4,128,128]{2,1,0:T(8,128)} %start_state.1, f32[1,512]{1,0:T(1,128)} %bitcast.6, f32[4096,8]{1,0:T(8,128)} %copy.18.gates, ...), custom_call_target="tpu_custom_call" | custom-call | tf_op jit(solution)/shard_map/pallas_call | solution.py:359
  81.7 1.9 %copy.20 = bf16[256,1024]{1,0:T(8,128)(2,1)} copy(bf16[256,1024]{1,0:T(8,128)(2,1)} %shard_map.154) | data formatting | bytes 1048576

commit v2 on v1

v2 whole, which is shorter than its diff:
```python
import functools
import math

import jax
import jax.numpy as jnp
from jax import lax
from jax.experimental import pallas as pl
from jax.experimental.pallas import tpu as pltpu
from jax.sharding import PartitionSpec as P

FD = 64
KD = 128
EPSILON = 1e-06
BLOCK = 32
MESH = pl.DeviceIdType.MESH
F32 = jnp.float32
BF16 = jnp.bfloat16


def dot(a, b, ca=1, cb=0):
    return lax.dot_general(a, b, (((ca,), (cb,)), ((), ())), preferred_element_type=F32)


def layer_kernel(
    dims,
    tokens, gain, gate_floor, extra_decay, start_state, recur_gain, gates, attend_gain,
    w_ak, w_av, w_aq, w_rq, w_rf, w_rv, w_ro, w_ao,
    out,
    wbuf, wout, tok_all, scaled, proj, kv_all, q_all, m_ref, l_ref, acc, part, part_l,
    comb, comb_l, cum_ref, qe, rec_o, mix, st_all, chain_out, chain_in, rec_all, att_all,
    out_acc, q_aug, k_aug,
    w_sem, wo_sem, tok_s, tok_r, q_s, q_r, st_s, st_r, kv_s, kv_r, ch_s, ch_r,
    po_s, po_r, pl_s, pl_r, rr_s, rr_r, ra_s, ra_r,
):
    Z, G, TP, NG = dims
    rows, width = tokens.shape[0], recur_gain.shape[1]
    part_w = tokens.shape[1]
    model = part_w * TP
    rec_heads, att_heads = width // KD, width // FD
    HG, WG = att_heads // NG, width // NG
    c, t = lax.axis_index("sp"), lax.axis_index("tp")
    z, i = c // G, c % G

    loads = [
        pltpu.make_async_copy(w, wbuf.at[k], w_sem.at[k])
        for k, w in enumerate((w_ak, w_av, w_aq, w_rq, w_rf, w_rv))
    ]
    out_loads = [
        pltpu.make_async_copy(w, wout.at[k], wo_sem.at[k]) for k, w in enumerate((w_ro, w_ao))
    ]
    for load in loads[:3]:
        load.start()

    barrier = pltpu.get_barrier_semaphore()
    tp_peers = [(c, (t + d) % TP) for d in range(1, TP)]
    inner_peers = [(z * G + (i + d) % G, t) for d in range(1, G)]
    outer_peers = [(((z + d) % Z) * G + i, t) for d in range(1, Z)]
    for peer in tp_peers + inner_peers + outer_peers:
        pl.semaphore_signal(barrier, inc=1, device_id=peer, device_id_type=MESH)
    pl.semaphore_wait(barrier, TP - 1 + G - 1 + Z - 1)

    def remote(src, dst, s, r, peer):
        return pltpu.make_async_remote_copy(
            src_ref=src, dst_ref=dst, send_sem=s, recv_sem=r, device_id=peer, device_id_type=MESH
        )

    tok_copies = [
        remote(tokens, tok_all.at[t], tok_s.at[d], tok_r.at[d], peer)
        for d, peer in enumerate(tp_peers)
    ]
    for copy in tok_copies:
        copy.start()
    for load in loads[3:] + out_loads:
        load.start()
    tok_all[t] = tokens[...]
    for copy in tok_copies:
        copy.wait_recv()
    squares = jnp.zeros((rows, 1), F32)
    for p in range(TP):
        x = tok_all[p].astype(F32)
        squares = squares + jnp.sum(x * x, axis=1, keepdims=True)
        scaled[:, p * part_w:(p + 1) * part_w] = (x * gain[p]).astype(BF16)
    inverse = lax.rsqrt(squares / model + EPSILON)

    def project(k):
        return dot(scaled[...], wbuf[k]) * inverse

    loads[2].wait()
    turned_query = (project(2) * FD ** (-0.5)).T.astype(BF16)
    for g in range(NG):
        q_all[i, g] = turned_query[g * WG:(g + 1) * WG]

    def q_copies(g):
        return [
            remote(q_all.at[i, g], q_all.at[i, g], q_s.at[d, g], q_r.at[d, g], peer)
            for d, peer in enumerate(inner_peers)
        ]

    for g in range(NG):
        for copy in q_copies(g):
            copy.start()
    loads[0].wait()
    loads[1].wait()

    def project_kv(k, carry):
        turned = project(k).T.astype(BF16)
        for g in range(NG):
            kv_all[z, g, k] = turned[g * WG:(g + 1) * WG]
        return carry

    lax.fori_loop(0, 2, project_kv, 0)

    def kv_copy(slot, g):
        ref = kv_all.at[slot, g]
        return remote(ref, ref, kv_s.at[slot, g], kv_r.at[slot, g], (c + G, t))

    last = z == Z - 1

    @pl.when(jnp.logical_not(last))
    def _():
        for g in range(NG):
            kv_copy(z, g).start()

    for k in range(3, 6):
        loads[k].wait()

    def project_rec(k, carry):
        proj[k - 3] = project(k).astype(BF16)
        return carry

    lax.fori_loop(3, 6, project_rec, 0)

    rows_i = lax.broadcasted_iota(jnp.int32, (rows, rows), 0)
    cols_i = lax.broadcasted_iota(jnp.int32, (rows, rows), 1)
    lower = (cols_i <= rows_i).astype(F32).astype(BF16)
    extra = extra_decay[...].T
    for h in range(rec_heads):
        lanes = slice(h * KD, (h + 1) * KD)
        query = proj[0, :, lanes].astype(F32)
        value = proj[2, :, lanes]
        inflow = (1.0 - gate_floor[:, lanes]) * jax.nn.sigmoid(-proj[1, :, lanes].astype(F32))
        decay = jnp.log1p(-inflow) - extra[:, h:h + 1]
        high = decay.astype(BF16)
        rest = decay - high.astype(F32)
        mid = rest.astype(BF16)
        low = (rest - mid.astype(F32)).astype(BF16)
        cum_ref[...] = dot(lower, high) + (dot(lower, mid) + dot(lower, low))
        cum = cum_ref[...]
        qe[:, lanes] = (query * jnp.exp(cum)).astype(BF16)
        end = cum[rows - 1:rows]
        key_end = (inflow * jnp.exp(end - cum)).astype(BF16)
        st_all[i, h, :KD] = dot(value, key_end, 0, 0).astype(BF16)
        st_all[i, h, KD:] = jnp.broadcast_to(jnp.exp(end), (16, KD)).astype(BF16)
        mix[...] = jnp.zeros_like(mix)
        for b in range(rows // BLOCK):
            low_r, high_r = b * BLOCK, (b + 1) * BLOCK
            middle = cum[low_r + BLOCK // 2 - 1:low_r + BLOCK // 2]
            qb = (query[low_r:high_r] * jnp.exp(cum[low_r:high_r] - middle)).astype(BF16)
            kb = (inflow[:high_r] * jnp.exp(middle - cum[:high_r])).astype(BF16)
            a = dot(qb, kb, 1, 1)
            row_at = low_r + lax.broadcasted_iota(jnp.int32, a.shape, 0)
            col_at = lax.broadcasted_iota(jnp.int32, a.shape, 1)
            mix[low_r:high_r, :high_r] = jnp.where(col_at <= row_at, a, 0.0)
        rec_o[:, lanes] = dot(mix[...].astype(BF16), value)

    st_copies = [
        remote(st_all.at[i], st_all.at[i], st_s.at[d], st_r.at[d], peer)
        for d, peer in enumerate(inner_peers)
    ]
    for copy in st_copies:
        copy.start()

    m_ref[...] = jnp.full_like(m_ref, -1e30)
    l_ref[...] = jnp.zeros_like(l_ref)
    acc[...] = jnp.zeros_like(acc)
    q_aug[:, :, FD:, :] = jnp.ones((G, att_heads, FD, rows), BF16)

    row_at = lax.broadcasted_iota(jnp.int32, (FD, rows), 0)

    def widen_queries(g, j):
        for n in range(HG):
            q_aug[j, g * HG + n, :FD, :] = q_all[j, g, n * FD:(n + 1) * FD, :]

    def widen_keys(slot, g):
        key_gates = gates[:, pl.ds(pl.multiple_of((slot * G + i) * rows, rows), rows)]
        first = gates[:, pl.ds(pl.multiple_of(z * G * rows, rows), 128)][:, :1]
        bias = first - key_gates
        for n in range(HG):
            row = bias[g * HG + n:g * HG + n + 1]
            high = row.astype(BF16).astype(F32)
            mid = (row - high).astype(BF16).astype(F32)
            low = row - high - mid
            pieces = jnp.where(row_at == 0, high, jnp.where(row_at == 1, mid, low))
            pieces = jnp.where(row_at < 3, pieces, 0.0)
            keys = kv_all[slot, g, 0, n * FD:(n + 1) * FD, :].astype(F32)
            k_aug[n] = jnp.concatenate([keys, pieces], axis=0).T.astype(BF16)

    def attend(slot, g, j, diagonal):
        for n in range(HG):
            h = g * HG + n
            span, local = slice(h * FD, (h + 1) * FD), slice(n * FD, (n + 1) * FD)
            s = dot(k_aug[n], q_aug[j, h])
            if diagonal:
                s = jnp.where(rows_i <= cols_i, s, -1e30)
            before = m_ref[j, g, n:n + 1, :]
            top = jnp.maximum(before, jnp.max(s, axis=0, keepdims=True))
            w = jnp.exp(s - top)
            fade = jnp.exp(before - top)
            m_ref[j, g, n:n + 1, :] = top
            l_ref[j, g, n:n + 1, :] = l_ref[j, g, n:n + 1, :] * fade + jnp.sum(
                w, axis=0, keepdims=True
            )
            acc[j, span, :] = acc[j, span, :] * fade + dot(
                kv_all[slot, g, 1, local, :], w.astype(BF16)
            )

    def part_copies(d, g):
        j = (i + d) % G
        peer = (z * G + j, t)
        return (
            remote(part.at[j, g], comb.at[i, g], po_s.at[d, g], po_r.at[d, g], peer),
            remote(part_l.at[j, g], comb_l.at[i, g], pl_s.at[d, g], pl_r.at[d, g], peer),
        )

    def finish(d, g):
        j = (i + d) % G
        total = jnp.maximum(l_ref[j, g], 1e-30)
        part_l[j, g] = m_ref[j, g] + jnp.log(total)
        for n in range(HG):
            h = g * HG + n
            part[j, g, n * FD:(n + 1) * FD, :] = (
                acc[j, h * FD:(h + 1) * FD, :] / total[n:n + 1]
            ).astype(BF16)

        @pl.when(d < G)
        def _():
            for copy in part_copies(d, g):
                copy.start()

    def finish_all(g):
        def one(d, carry):
            finish(d, g)
            return carry

        lax.fori_loop(1, G + 1, one, 0)

    def group(g):
        widen_queries(g, i)
        widen_keys(z, g)
        attend(z, g, i, True)
        for copy in q_copies(g):
            copy.wait_recv()
        for d in range(1, G):
            widen_queries(g, (i + d) % G)

        def own_slot(d, carry):
            j = (i + d) % G

            @pl.when(j > i)
            def _():
                attend(z, g, j, False)

            return carry

        lax.fori_loop(1, G, own_slot, 0)

        def earlier_slot(n, carry):
            slot = z - n
            kv_copy(slot, g).wait_recv()

            @pl.when(jnp.logical_not(last))
            def _():
                kv_copy(slot, g).start()

            widen_keys(slot, g)
            for j in range(G):
                attend(slot, g, j, False)
            return carry

        lax.fori_loop(1, z + 1, earlier_slot, 0)
        finish_all(g)

    def att_copies(g):
        return [
            remote(att_all.at[t, g], att_all.at[t, g], ra_s.at[d, g], ra_r.at[d, g], peer)
            for d, peer in enumerate(tp_peers)
        ]

    def combine(g):
        comb[i, g] = part[i, g]
        comb_l[i, g] = part_l[i, g]
        for d in range(1, G):
            for copy in part_copies(d, g):
                copy.wait_recv()
        top = comb_l[0, g]
        for k in range(1, G):
            top = jnp.maximum(top, comb_l[k, g])
        shares = [jnp.exp(comb_l[k, g] - top) for k in range(G)]
        whole = shares[0]
        for k in range(1, G):
            whole = whole + shares[k]
        for n in range(HG):
            span = slice(n * FD, (n + 1) * FD)
            x = jnp.zeros((FD, rows), F32)
            for k in range(G):
                x = x + comb[k, g, span, :].astype(F32) * (shares[k][n:n + 1] / whole[n:n + 1])
            acc[0, span, :] = x * lax.rsqrt(jnp.mean(x * x, axis=0, keepdims=True) + EPSILON)
        att_all[t, g] = (acc[0, :WG].T * attend_gain[:, g * WG:(g + 1) * WG]).astype(BF16)
        for copy in att_copies(g):
            copy.start()

    half = max(1, NG - 1)
    for g in range(half):
        with jax.named_scope(f"group{g}"):
            group(g)

    for copy in st_copies:
        copy.wait_recv()
    chain_copy = remote(chain_out, chain_in, ch_s, ch_r, (c + G, t))

    @pl.when(z == 0)
    def _():
        for h in range(rec_heads):
            chain_in[h] = start_state[h].T.astype(BF16)

    @pl.when(z > 0)
    def _():
        chain_copy.wait_recv()

    for h in range(rec_heads):
        lanes = slice(h * KD, (h + 1) * KD)

        def pass_on(k, state):
            return st_all[k, h, KD:KD + 1].astype(F32) * state + st_all[k, h, :KD].astype(F32)

        state = lax.fori_loop(0, i, pass_on, chain_in[h].astype(F32))
        chain_out[h] = lax.fori_loop(i, G, pass_on, state).astype(BF16)
        rec_o[:, lanes] = rec_o[:, lanes] + dot(qe[:, lanes], state.astype(BF16), 1, 1)

    @pl.when(jnp.logical_not(last))
    def _():
        chain_copy.start()

    for h in range(rec_heads):
        lanes = slice(h * KD, (h + 1) * KD)
        x = rec_o[:, lanes]
        x = x * lax.rsqrt(jnp.mean(x * x, axis=1, keepdims=True) + EPSILON)
        rec_all[t, :, lanes] = (x * recur_gain[:, lanes]).astype(BF16)
    rec_copies = [
        remote(rec_all.at[t], rec_all.at[t], rr_s.at[d], rr_r.at[d], peer)
        for d, peer in enumerate(tp_peers)
    ]
    for copy in rec_copies:
        copy.start()

    for g in range(half, NG):
        with jax.named_scope(f"group{g}"):
            group(g)

    tile = min(256, out.shape[1])

    def output(first, groups, ends):
        def columns_of(n, carry):
            columns = pl.ds(pl.multiple_of(n * tile, tile), tile)
            total = jnp.zeros((rows, tile), F32) if first else out_acc[:, columns]
            for p in range(TP):
                if first:
                    total = total + dot(rec_all[p], wout[0, p * width:(p + 1) * width, columns])
                for g in groups:
                    start = p * width + g * WG
                    total = total + dot(att_all[p, g], wout[1, start:start + WG, columns])
            if ends:
                out[:, columns] = total.astype(BF16)
            else:
                out_acc[:, columns] = total
            return carry

        lax.fori_loop(0, out.shape[1] // tile, columns_of, 0)

    with jax.named_scope("combine_a"):
        for g in range(NG - 1):
            combine(g)
        for load in out_loads:
            load.wait()
        for copy in rec_copies:
            copy.wait_recv()
        output(True, (), False)
    with jax.named_scope("combine_b"):
        combine(NG - 1)
    with jax.named_scope("last"):
        for g in range(NG):
            for copy in att_copies(g):
                copy.wait_recv()
        output(False, range(NG), True)

    for copy in tok_copies + st_copies + rec_copies:
        copy.wait_send()
    for g in range(NG):
        for copy in att_copies(g) + q_copies(g):
            copy.wait_send()
        for d in range(1, G):
            for copy in part_copies(d, g):
                copy.wait_send()

    @pl.when(jnp.logical_not(last))
    def _():
        chain_copy.wait_send()

        def sent(n, carry):
            for g in range(NG):
                kv_copy(z - n, g).wait_send()
            return carry

        lax.fori_loop(0, z + 1, sent, 0)


def shards(
    sizes, tokens, norm_gain, recur_query, recur_forget, recur_value, gate_floor, extra_decay,
    start_state, recur_gain, attend_query, attend_key, attend_value, gate_cache, attend_gain,
    recur_output, attend_output,
):
    sp, TP = sizes
    G = math.isqrt(sp)
    while sp % G:
        G -= 1
    Z = sp // G
    rows, part_w = tokens.shape
    width = recur_gain.shape[0]
    model = norm_gain.shape[0]
    rec_heads, att_heads = width // KD, width // FD
    out_w = recur_output.shape[1]
    NG = math.gcd(att_heads, 4)
    HG, WG = att_heads // NG, width // NG
    vmem = pl.BlockSpec(memory_space=pltpu.VMEM)
    anywhere = pl.BlockSpec(memory_space=pl.ANY)
    dma = pltpu.SemaphoreType.DMA
    return pl.pallas_call(
        functools.partial(layer_kernel, (Z, G, TP, NG)),
        out_shape=jax.ShapeDtypeStruct((rows, out_w), BF16),
        in_specs=[vmem] * 8 + [anywhere] * 8,
        out_specs=vmem,
        scratch_shapes=[
            pltpu.VMEM((6, model, width), BF16),
            pltpu.VMEM((2, width * TP, out_w), BF16),
            pltpu.VMEM((TP, rows, part_w), BF16),
            pltpu.VMEM((rows, model), BF16),
            pltpu.VMEM((3, rows, width), BF16),
            pltpu.VMEM((Z, NG, 2, WG, rows), BF16),
            pltpu.VMEM((G, NG, WG, rows), BF16),
            pltpu.VMEM((G, NG, HG, rows), F32),
            pltpu.VMEM((G, NG, HG, rows), F32),
            pltpu.VMEM((G, width, rows), F32),
            pltpu.VMEM((G, NG, WG, rows), BF16),
            pltpu.VMEM((G, NG, HG, rows), F32),
            pltpu.VMEM((G, NG, WG, rows), BF16),
            pltpu.VMEM((G, NG, HG, rows), F32),
            pltpu.VMEM((rows, KD), F32),
            pltpu.VMEM((rows, width), BF16),
            pltpu.VMEM((rows, width), F32),
            pltpu.VMEM((rows, rows), F32),
            pltpu.VMEM((G, rec_heads, KD + 16, KD), BF16),
            pltpu.VMEM((rec_heads, KD, KD), BF16),
            pltpu.VMEM((rec_heads, KD, KD), BF16),
            pltpu.VMEM((TP, rows, width), BF16),
            pltpu.VMEM((TP, NG, rows, WG), BF16),
            pltpu.VMEM((rows, out_w), F32),
            pltpu.VMEM((G, att_heads, 2 * FD, rows), BF16),
            pltpu.VMEM((HG, rows, 2 * FD), BF16),
            dma((6,)), dma((2,)),
            dma((TP,)), dma((TP,)),
            dma((G, NG)), dma((G, NG)), dma((G,)), dma((G,)),
            dma((Z, NG)), dma((Z, NG)), dma, dma,
            dma((G, NG)), dma((G, NG)), dma((G, NG)), dma((G, NG)),
            dma((TP,)), dma((TP,)), dma((TP, NG)), dma((TP, NG)),
        ],
        compiler_params=pltpu.CompilerParams(
            collective_id=0, has_side_effects=True, vmem_limit_bytes=56 * 1024 * 1024
        ),
    )(
        tokens, norm_gain.reshape(TP, 1, part_w), gate_floor.reshape(1, width), extra_decay.T,
        start_state, recur_gain.reshape(1, width), gate_cache.T, attend_gain.reshape(1, width),
        attend_key, attend_value, attend_query, recur_query, recur_forget, recur_value,
        recur_output, attend_output,
    )


def solution(mesh):
    sizes = (mesh.shape["sp"], mesh.shape["tp"])
    return jax.shard_map(
        functools.partial(shards, sizes),
        mesh=mesh,
        in_specs=(
            P("sp", "tp"),
            P(),
            P(None, "tp"),
            P(None, "tp"),
            P(None, "tp"),
            P("tp"),
            P("sp", "tp"),
            P("tp", None, None),
            P("tp"),
            P(None, "tp"),
            P(None, "tp"),
            P(None, "tp"),
            P(None, "tp"),
            P("tp"),
            P(None, "tp"),
            P(None, "tp"),
        ),
        out_specs=P("sp", "tp"),
        check_vma=False,
    )
```

time: 83.8 us -> 73.6 us (0.88)
  Pallas kernels: 77.3 us -> 71.5 us
  local copies, waits for them, and re-layouts: 6.21 us -> 1.87 us
    pallas_call x1, Pallas kernels: 77.3 us -> 71.5 us  [shards(): pl.pallas_call(functools.partial(layer_kernel, (Z, G, TP, NG)), out_shape...]
    unnamed x3 -> x1, local copies, waits for them, and re-layouts: 6.21 us -> 1.87 us
where the time goes in v2:
time: 73.6 us; the launch traced here: 73.4 us
  Pallas kernels  71.5 us (97%)
  local copies, waits for them, and re-layouts  1.87 us (3%)
    pallas_call x1, Pallas kernels, shards(): pl.pallas_call(functools.partial(layer_kernel, (Z, G, TP, NG)), out_shape...  71.5 us
    unnamed x1, local copies, waits for them, and re-layouts  1.87 us

profile of v2, /device:TPU:31, one launch (start us, length us, event | category | flops | bytes accessed | tf_op | source)
XLA Modules:
  0.0 73.4 jit_solution(13132634638554068449)
XLA Ops:
  0.0 71.5 %shard_map.154 = bf16[256,1024]{1,0:T(8,128)(2,1)} custom-call(bf16[256,1024]{1,0:T(8,128)(2,1)} %tokens.1, f32[2,1,1024]{2,1,0:T(1,128)} %bitcast.7, f32[1,512]{1,0:T(1,128)} %bitcast.9, f32[4,256]{1,0:T(4,128)} %bitcast.8, f32[4,128,128]{2,1,0:T(8,128)} %start_state.1, f32[1,512]{1,0:T(1,128)} %bitcast.10, f32[8,4096]{1,0:T(8,128)} %bitcast.6, ...), custom_call_target="tpu_custom_call" | custom-call | tf_op jit(solution)/shard_map/pallas_call | solution.py:437
  71.5 1.9 %copy.18 = bf16[256,1024]{1,0:T(8,128)(2,1)} copy(bf16[256,1024]{1,0:T(8,128)(2,1)} %shard_map.154) | data formatting | bytes 1048576
